TPU v7x, 32 devices: a whole 2x2x4 slice. The times are simulated.
32 devices in a mesh: ep: 8 (over z, x), tp: 4 (over y, core).
Axes of the slice: x: 2, y: 2, z: 4, core: 2. Of those that a mesh axis runs over, the one named last changes fastest.
Arguments:
- queries: bfloat16 [4096, 2048], P('ep', 'tp'), may hold values from -6 to 6
- keys_values: bfloat16 [4096, 4, 128], P('ep', 'tp'), may hold values from -12 to 12
- sinks: float32 [32], P('tp'), may hold values from 1 to 5
- tokens_b: bfloat16 [4096, 2048], P(('ep', 'tp')), may hold values from -6 to 6
- norm_gain: float32 [2048], replicated, may hold values from 0.1 to 1.9
- routes: int32 [4096, 2], P(('ep', 'tp')), may hold values from 0 to 7, all different within a row; in each aligned block of 128 rows (0 to 127, 128 to 255, ...) at most 40 rows name the same one
- route_weights: float32 [4096, 2], P(('ep', 'tp')), may hold values from 0.1 to 0.9
- gate_weight: bfloat16 [8, 2048, 3584], P('ep', None, 'tp'), may hold values from -0.125 to 0.125
- up_weight: bfloat16 [8, 2048, 3584], P('ep', None, 'tp'), may hold values from -0.125 to 0.125
- down_weight: bfloat16 [8, 3584, 2048], P('ep', 'tp'), may hold values from -0.09375 to 0.09375
Outputs:
- attended: bfloat16 [4096, 2048], P('ep', 'tp')
- moe_out: bfloat16 [4096, 2048], P(('ep', 'tp'))
Inputs may be any that keep to these rules, and one draw needn't show every extreme that they name: `routes`: in each aligned block of 128 rows (the rows of one device) no expert is named by more than 40 rows; the 2 entries of a row differ.
All inputs are finite; a program needn't handle non-finite values.
Results may differ from a plain program's by a relative error of at most 0.012.
Values may be sent and summed in bfloat16 or wider, within the bound.
A program may use at most 128 MiB of HBM per device.

v0:
```python
import functools

import jax
import jax.numpy as jnp
from jax import lax
from jax.experimental import pallas as pl
from jax.experimental.pallas import tpu as pltpu
from jax.sharding import PartitionSpec as P

WINDOW = 128
EPSILON = 1e-06
GROUPS = 8
LATE = 2
MESH = pl.DeviceIdType.MESH
F32 = jnp.float32
BF16 = jnp.bfloat16


def remote(src, dst, send_sem, recv_sem, device):
    return pltpu.make_async_remote_copy(
        src_ref=src, dst_ref=dst, send_sem=send_sem, recv_sem=recv_sem,
        device_id=device, device_id_type=MESH,
    )


def kernel(
    n, m, cap, slot_rows,
    q_hbm, kv_hbm, sink_ref, tok_ref, gain_ref, routes_ref, rw_ref, wg_hbm, wu_hbm, wd_hbm,
    att_ref, moe_ref,
    q_ref, wg, wu, wd, kvx, out, piece, xb, hidden, parts, ra, qb, rb, fin, ret, comb,
    w_sem, halo_sem, ep_send, ep_recv, y_send, y_recv, c_send, c_recv, d_send, d_recv,
    a_send, a_recv, b_send, b_recv, r_send, r_recv,
):
    p = lax.axis_index("ep")
    t = lax.axis_index("tp")
    t1 = t + 1 - 2 * (t % 2)
    t2 = (t + m // 2) % m
    t3 = (t1 + m // 2) % m
    per = n // GROUPS
    rows = m * per * slot_rows
    width = tok_ref.shape[1]
    hid = wg.shape[1]
    row_count = q_ref.shape[0]
    blocks = row_count // WINDOW

    def xor(a, b):
        total, bit = 0, 1
        while bit < n:
            total = total + ((a // bit + b // bit) % 2) * bit
            bit *= 2
        return total

    loads = [
        pltpu.make_async_copy(wg_hbm, wg, w_sem.at[0]),
        pltpu.make_async_copy(wu_hbm, wu, w_sem.at[1]),
        pltpu.make_async_copy(wd_hbm, wd, w_sem.at[2]),
    ]
    q_load = pltpu.make_async_copy(q_hbm, q_ref, w_sem.at[3])
    kv_load = pltpu.make_async_copy(kv_hbm, kvx.at[pl.ds(WINDOW, row_count)], w_sem.at[4])
    barrier = pltpu.get_barrier_semaphore()
    for s in range(1, n):
        pl.semaphore_signal(barrier, inc=1, device_id=(xor(p, s), t), device_id_type=MESH)
    pl.semaphore_signal(barrier, inc=1, device_id=(p, t1), device_id_type=MESH)
    pl.semaphore_signal(barrier, inc=1, device_id=(p, t2), device_id_type=MESH)

    kv_load.start()
    q_load.start()
    for load in loads:
        load.start()

    widened = tok_ref[...].astype(F32)
    scale = lax.rsqrt(jnp.mean(widened * widened, axis=-1, keepdims=True) + EPSILON)
    normed = (widened * scale * gain_ref[...]).astype(BF16)

    own = normed.shape[0]
    r0 = routes_ref[0:1, :]
    r1 = routes_ref[1:2, :]
    ids = lax.broadcasted_iota(jnp.int32, (max(n, 8), own), 0)
    is0 = ids == r0
    is1 = ids == r1
    member = jnp.where(is0 | is1, 1.0, 0.0).astype(BF16)
    rowi = lax.broadcasted_iota(jnp.int32, (own, own), 0)
    coli = lax.broadcasted_iota(jnp.int32, (own, own), 1)
    before = jnp.where(rowi < coli, 1.0, 0.0).astype(BF16)
    rank = jnp.dot(member, before, preferred_element_type=F32)
    k0 = jnp.sum(jnp.where(is0, rank, 0.0), axis=0, keepdims=True).astype(jnp.int32)
    k1 = jnp.sum(jnp.where(is1, rank, 0.0), axis=0, keepdims=True).astype(jnp.int32)
    e0 = jnp.bitwise_xor(r0, p) * slot_rows + k0
    e1 = jnp.bitwise_xor(r1, p) * slot_rows + k1
    slots = n * slot_rows
    slot_i = lax.broadcasted_iota(jnp.int32, (slots, own), 0)
    in0 = slot_i == e0
    in1 = slot_i == e1
    pick = jnp.where(in0 | in1, 1.0, 0.0).astype(BF16)
    weight = jnp.where(in0, rw_ref[0:1, :], 0.0) + jnp.where(in1, rw_ref[1:2, :], 0.0)
    high = weight.astype(BF16)
    comb[0] = high
    comb[1] = (weight - high.astype(F32)).astype(BF16)
    def dispatch(s):
        return remote(out.at[s], piece.at[t, s], ep_send.at[s], ep_recv.at[s], (xor(p, s), t))

    def halo(to):
        return remote(kvx.at[pl.ds(row_count, WINDOW)], kvx.at[pl.ds(0, WINDOW)], halo_sem.at[0], halo_sem.at[1], (to, t))

    def part(g):
        return pl.ds(g * per, per)

    def y_copy(g):
        return remote(piece.at[t, part(g)], piece.at[t, part(g)], y_send.at[g], y_recv.at[g], (p, t2))

    def c_copy(g):
        return remote(piece.at[t, part(g)], piece.at[t, part(g)], c_send.at[g], c_recv.at[g], (p, t1))

    tile = min(512, width)
    for c in range(0, width, tile):
        block = jnp.dot(pick, normed[:, c : c + tile], preferred_element_type=F32)
        for s in range(n):
            out[s, :, c : c + tile] = block[s * slot_rows : (s + 1) * slot_rows].astype(BF16)
    piece[t, 0] = out[0]

    pl.semaphore_wait(barrier, n + 1)

    kv_load.wait()

    @pl.when(p < n - 1)
    def _():
        halo(p + 1).start()

    @pl.loop(1, n)
    def _(s):
        dispatch(s).start()

    if per == 1:
        y_copy(0).start()
        c_copy(0).start()

    q_load.wait()

    @pl.when(p == 0)
    def _():
        kvx[0:WINDOW, :] = jnp.zeros((WINDOW, kvx.shape[1]), BF16)

    def d_copy(g):
        return remote(piece.at[t2, part(g)], piece.at[t2, part(g)], d_send.at[g], d_recv.at[g], (p, t1))

    def a_copy(i, g):
        return remote(parts.at[(t1, t3)[i], part(g)], ra.at[i, part(g)], a_send.at[i, g], a_recv.at[i, g], (p, t1))

    def b_copy(g):
        return remote(qb.at[part(g)], rb.at[part(g)], b_send.at[g], b_recv.at[g], (p, t2))

    def back(s):
        return remote(fin.at[s], ret.at[s], r_send.at[s], r_recv.at[s], (xor(p, s), t))

    def attention(b):
        head = kvx.shape[1] // 2
        local_heads = q_ref.shape[1] // head
        heads = local_heads * m
        near = kvx[pl.ds(pl.multiple_of(b * WINDOW, WINDOW), 2 * WINDOW), :]
        keys = (near[:, :head].astype(F32) * head ** (-0.5)).astype(BF16)
        ones = jnp.ones((2 * WINDOW, head), BF16)
        values = jnp.concatenate([near[:, head:], ones], axis=1)
        qi = lax.broadcasted_iota(jnp.int32, (WINDOW, 2 * WINDOW), 0)
        kj = lax.broadcasted_iota(jnp.int32, (WINDOW, 2 * WINDOW), 1)
        dist = WINDOW + qi - kj
        first = jnp.where(p + b == 0, WINDOW, 0)
        allowed = (dist >= 0) & (dist < WINDOW) & (kj >= first)
        dist_f = dist.astype(F32)
        at = pl.ds(pl.multiple_of(b * WINDOW, WINDOW), WINDOW)
        for pair in range(0, local_heads, 2):
            both = q_ref[at, pair * head : (pair + 2) * head]
            done = []
            for i in range(2):
                h = pair + i
                scores = lax.dot_general(
                    both[:, i * head : (i + 1) * head], keys, (((1,), (1,)), ((), ())),
                    preferred_element_type=F32,
                )
                ids = jnp.full((1, 2 * WINDOW), t * local_heads + h + 1, jnp.int32).astype(F32)
                slope = jnp.exp2(ids * (-8.0 / heads))
                scores = jnp.where(allowed, scores - slope * dist_f, -1e30)
                sink = sink_ref[h]
                peak = jnp.maximum(jnp.max(scores, axis=-1, keepdims=True), sink)
                weights = jnp.exp(scores - peak).astype(BF16)
                mixed = jnp.dot(weights, values, preferred_element_type=F32)
                total = mixed[:, head : head + 1] + jnp.exp(sink - peak)
                done.append(mixed[:, :head] / total)
            att_ref[at, pair * head : (pair + 2) * head] = jnp.concatenate(done, axis=1).astype(BF16)

    def experts(g):
        for o in range(m):
            for j in range(0, per):
                k = (o * per + j) * slot_rows
                xb[k : k + slot_rows, :] = piece[o, g * per + j]
        full = hid // 256 * 256
        x = xb[...]
        for c in range(0, full, 256):
            gate = jnp.dot(x, wg[:, c : c + 256], preferred_element_type=F32)
            up = jnp.dot(x, wu[:, c : c + 256], preferred_element_type=F32)
            hidden[:, c : c + 256] = (gate / (1.0 + jnp.exp(-gate)) * up).astype(BF16)
        if full < hid:
            tail = hid - full
            joint = jnp.concatenate([wg[:, full:], wu[:, full:]], axis=1)
            two = jnp.dot(x, joint, preferred_element_type=F32)
            gate, up = two[:, :tail], two[:, tail:]
            hidden[:, full:] = (gate / (1.0 + jnp.exp(-gate)) * up).astype(BF16)
        h = hidden[...]
        for c in range(0, width, 256):
            product = jnp.dot(h, wd[:, c : c + 256], preferred_element_type=F32)
            for o in range(m):
                for j in range(per):
                    k = (o * per + j) * slot_rows
                    parts[o, g * per + j, :, c : c + 256] = product[k : k + slot_rows].astype(BF16)

    def finish(g):
        b_copy(g).wait_recv()
        for j in range(per):
            s = g * per + j
            fin[s] = (parts[t, s].astype(F32) + ra[0, s].astype(F32) + rb[s].astype(F32)).astype(BF16)

            @pl.when(s > 0)
            def _():
                back(s).start()

    def middle(g):
        a_copy(0, g).wait_recv()
        a_copy(1, g).wait_recv()
        for j in range(per):
            s = g * per + j
            qb[s] = (parts[t2, s].astype(F32) + ra[1, s].astype(F32)).astype(BF16)
        b_copy(g).start()

    @pl.loop(0, GROUPS + 2)
    def _(it):
        @pl.when((it < GROUPS) & (it >= (1 if per == 1 else 0)))
        def _():
            for j in range(per):
                s = it * per + j

                @pl.when(s > 0)
                def _():
                    dispatch(s).wait_recv()

            y_copy(it).start()
            c_copy(it).start()

        @pl.when((it >= 1) & (it <= GROUPS))
        def _():
            y_copy(it - 1).wait_recv()
            d_copy(it - 1).start()

        @pl.when(it >= 3 + LATE)
        def _():
            finish(it - 3)

        @pl.when((it >= 2 + LATE) & (it <= GROUPS + 1))
        def _():
            middle(it - 2)

        @pl.when(it < blocks)
        def _():
            @pl.when((it == blocks - 1) & (p > 0))
            def _():
                halo((p + 1) % n).wait_recv()

            attention(blocks - 1 - it)

        @pl.when(it == 1)
        def _():
            for load in loads:
                load.wait()

        @pl.when((it >= 1) & (it <= GROUPS))
        def _():
            g = it - 1
            c_copy(g).wait_recv()
            d_copy(g).wait_recv()
            experts(g)
            a_copy(0, g).start()
            a_copy(1, g).start()

    for g in reversed(range(LATE)):
        middle(g)
    finish(GROUPS - 1)
    for g in reversed(range(LATE)):
        finish(g)
    ret[0] = fin[0]

    @pl.loop(1, n)
    def _(s):
        back(s).wait_recv()

    across = (((0,), (0,)), ((), ()))
    for c in range(0, width, tile):
        flat = jnp.concatenate([ret[s, :, c : c + tile].astype(F32) for s in range(n)], axis=0).astype(BF16)
        moe_ref[:, c : c + tile] = (
            lax.dot_general(comb[0], flat, across, preferred_element_type=F32)
            + lax.dot_general(comb[1], flat, across, preferred_element_type=F32)
        ).astype(BF16)

    @pl.when(p < n - 1)
    def _():
        halo(p + 1).wait_send()

    @pl.loop(1, n)
    def _(s):
        dispatch(s).wait_send()
        back(s).wait_send()

    @pl.loop(0, GROUPS)
    def _(g):
        y_copy(g).wait_send()
        c_copy(g).wait_send()
        d_copy(g).wait_send()
        a_copy(0, g).wait_send()
        a_copy(1, g).wait_send()
        b_copy(g).wait_send()


def local(n, m, queries, keys_values, sinks, tokens_b, norm_gain, routes, route_weights, gate_weight, up_weight, down_weight):
    own_rows, top_count = routes.shape
    width = tokens_b.shape[1]
    cap = max(2, 5 * own_rows * top_count // (4 * n))
    slot_rows = (cap + 7) // 8 * 8
    hid = gate_weight.shape[2]
    per = n // GROUPS
    rows = m * per * slot_rows
    vmem = pl.BlockSpec(memory_space=pltpu.VMEM)
    smem = pl.BlockSpec(memory_space=pltpu.SMEM)
    hbm = pl.BlockSpec(memory_space=pltpu.HBM)
    dma = pltpu.SemaphoreType.DMA
    return pl.pallas_call(
        functools.partial(kernel, n, m, cap, slot_rows),
        out_shape=(
            jax.ShapeDtypeStruct(queries.shape, BF16),
            jax.ShapeDtypeStruct(tokens_b.shape, BF16),
        ),
        in_specs=[hbm, hbm, smem, vmem, vmem, vmem, vmem, hbm, hbm, hbm],
        out_specs=(vmem, vmem),
        scratch_shapes=[
            pltpu.VMEM(queries.shape, BF16),
            pltpu.VMEM((width, hid), BF16),
            pltpu.VMEM((width, hid), BF16),
            pltpu.VMEM((hid, width), BF16),
            pltpu.VMEM((keys_values.shape[0] + WINDOW, keys_values.shape[2]), BF16),
            pltpu.VMEM((n, slot_rows, width), BF16),
            pltpu.VMEM((m, n, slot_rows, width), BF16),
            pltpu.VMEM((rows, width), BF16),
            pltpu.VMEM((rows, hid), BF16),
            pltpu.VMEM((m, n, slot_rows, width), BF16),
            pltpu.VMEM((2, n, slot_rows, width), BF16),
            pltpu.VMEM((n, slot_rows, width), BF16),
            pltpu.VMEM((n, slot_rows, width), BF16),
            pltpu.VMEM((n, slot_rows, width), BF16),
            pltpu.VMEM((n, slot_rows, width), BF16),
            pltpu.VMEM((2, n * slot_rows, own_rows), BF16),
            dma((5,)), dma((2,)), dma((n,)), dma((n,)),
            dma((GROUPS,)), dma((GROUPS,)), dma((GROUPS,)), dma((GROUPS,)), dma((GROUPS,)), dma((GROUPS,)),
            dma((2, GROUPS)), dma((2, GROUPS)), dma((GROUPS,)), dma((GROUPS,)), dma((n,)), dma((n,)),
        ],
        compiler_params=pltpu.CompilerParams(
            collective_id=0, has_side_effects=True, vmem_limit_bytes=62 * 1024 * 1024
        ),
    )(
        queries,
        keys_values.reshape(keys_values.shape[0], keys_values.shape[2]),
        sinks,
        tokens_b,
        norm_gain.reshape(1, width),
        routes.T,
        route_weights.T,
        gate_weight.reshape(width, hid),
        up_weight.reshape(width, hid),
        down_weight.reshape(hid, width),
    )


def solution(mesh):
    in_specs = (
        P("ep", "tp"),
        P("ep", "tp", None),
        P("tp"),
        P(("ep", "tp"), None),
        P(),
        P(("ep", "tp"), None),
        P(("ep", "tp"), None),
        P("ep", None, "tp"),
        P("ep", None, "tp"),
        P("ep", "tp", None),
    )
    out_specs = (P("ep", "tp"), P(("ep", "tp"), None))
    body = functools.partial(local, mesh.shape["ep"], mesh.shape["tp"])
    return jax.shard_map(body, mesh=mesh, in_specs=in_specs, out_specs=out_specs, check_vma=False)
```

profile of v0, /device:TPU:0, one launch (start us, length us, event | category | flops | bytes accessed | tf_op | source)
XLA Modules:
  0.0 85.7 jit_solution(2563626054445584263)
XLA Ops:
  0.6 81.3 %shard_map.113 = (bf16[512,512]{1,0:T(8,128)(2,1)}, bf16[128,2048]{1,0:T(8,128)(2,1)}) custom-call(bf16[512,512]{1,0:T(8,128)(2,1)} %q_hbm.1, bf16[512,128]{1,0:T(8,128)(2,1)} %bitcast.10, f32[8]{0:T(128)} %sink_ref.1, bf16[128,2048]{1,0:T(8,128)(2,1)} %tok_ref.1, f32[1,2048]{1,0:T(1,128)} %bitcast.11, s32[2,128]{1,0:T(2,128)} %bitcast.12, ...), custom_call_target="tpu_custom_call" | custom-call | tf_op jit(solution)/shard_map/pallas_call | solution.py:332
  81.9 1.9 %copy.14 = bf16[512,512]{1,0:T(8,128)(2,1)} copy(bf16[512,512]{1,0:T(8,128)(2,1)} %get-tuple-element.4) | data formatting | bytes 1048576
  83.8 1.9 %copy.15 = bf16[128,2048]{1,0:T(8,128)(2,1)} copy(bf16[128,2048]{1,0:T(8,128)(2,1)} %get-tuple-element.5) | data formatting | bytes 1048576
where the time goes:
time: 87 us; the launch traced here: 85.7 us
  Pallas kernels  81.3 us (93%)
  local copies, waits for them, and re-layouts  3.75 us (4%)
    pallas_call x1, Pallas kernels, local(): pl.pallas_call(functools.partial(kernel, n, m, cap, slot_rows), out_shape...  81.3 us
    unnamed x2, local copies, waits for them, and re-layouts  3.75 us

commit v1 on v0

--- a/solution.py
+++ b/solution.py
@@ -10,7 +10,19 @@
 WINDOW = 128
 EPSILON = 1e-06
 GROUPS = 8
-LATE = 2
+SEND = (0, 1, 4, 5, 2, 6, 3, 7)
+ORDER = (0, 1, 4, 2, 5, 3, 6, 7)
+PLAN = (
+    ("Y1", "F0"),
+    ("Y4", "F1", "M0"),
+    ("Y2", "F4"),
+    ("Y5", "F2", "M4", "R0"),
+    ("Y3", "F5"),
+    ("Y6", "R4", "M5", "F3"),
+    ("Y7", "F6"),
+    ("R5", "M6", "M1", "F7"),
+)
+TAIL = ("R6", "M7", "M3", "M2", "R1", "R7", "K0", "K4", "R3", "K5", "R2", "K6", "K1", "K7", "K3", "K2")
 MESH = pl.DeviceIdType.MESH
 F32 = jnp.float32
 BF16 = jnp.bfloat16
@@ -26,9 +38,9 @@
 def kernel(
     n, m, cap, slot_rows,
     q_hbm, kv_hbm, sink_ref, tok_ref, gain_ref, routes_ref, rw_ref, wg_hbm, wu_hbm, wd_hbm,
-    att_ref, moe_ref,
-    q_ref, wg, wu, wd, kvx, out, piece, xb, hidden, parts, ra, qb, rb, fin, ret, comb,
-    w_sem, halo_sem, ep_send, ep_recv, y_send, y_recv, c_send, c_recv, d_send, d_recv,
+    att_hbm, moe_hbm,
+    att_ref, moe_ref, acc, q_ref, wg, wu, wd, kvx, out, piece, xb, hidden, parts, ra, qb, rb, fin, ret, comb,
+    o_sem, w_sem, halo_sem, ep_send, ep_recv, y_send, y_recv, c_send, c_recv, d_send, d_recv,
     a_send, a_recv, b_send, b_recv, r_send, r_recv,
 ):
     p = lax.axis_index("ep")
@@ -93,9 +105,8 @@
     in1 = slot_i == e1
     pick = jnp.where(in0 | in1, 1.0, 0.0).astype(BF16)
     weight = jnp.where(in0, rw_ref[0:1, :], 0.0) + jnp.where(in1, rw_ref[1:2, :], 0.0)
-    high = weight.astype(BF16)
-    comb[0] = high
-    comb[1] = (weight - high.astype(F32)).astype(BF16)
+    for s in range(n):
+        comb[s] = weight[s * slot_rows : (s + 1) * slot_rows].astype(BF16)
     def dispatch(s):
         return remote(out.at[s], piece.at[t, s], ep_send.at[s], ep_recv.at[s], (xor(p, s), t))
 
@@ -126,9 +137,9 @@
     def _():
         halo(p + 1).start()
 
-    @pl.loop(1, n)
-    def _(s):
-        dispatch(s).start()
+    for g in SEND:
+        for v in range(max(1, g * per), (g + 1) * per):
+            dispatch(v).start()
 
     if per == 1:
         y_copy(0).start()
@@ -212,91 +223,107 @@
                     k = (o * per + j) * slot_rows
                     parts[o, g * per + j, :, c : c + 256] = product[k : k + slot_rows].astype(BF16)
 
-    def finish(g):
-        b_copy(g).wait_recv()
-        for j in range(per):
-            s = g * per + j
-            fin[s] = (parts[t, s].astype(F32) + ra[0, s].astype(F32) + rb[s].astype(F32)).astype(BF16)
-
-            @pl.when(s > 0)
-            def _():
-                back(s).start()
+    across = (((0,), (0,)), ((), ()))
+    att_out = pltpu.make_async_copy(att_ref, att_hbm, o_sem.at[0])
+
+    def moe_out(i):
+        cols = pl.ds(i * tile, tile)
+        return pltpu.make_async_copy(moe_ref.at[:, cols], moe_hbm.at[:, cols], o_sem.at[1 + i])
+
+    def spread(g):
+        for v in range(max(1, g * per), (g + 1) * per):
+            dispatch(v).wait_recv()
+        y_copy(g).start()
+        c_copy(g).start()
+
+    def forward(g):
+        y_copy(g).wait_recv()
+        d_copy(g).start()
 
     def middle(g):
         a_copy(0, g).wait_recv()
         a_copy(1, g).wait_recv()
-        for j in range(per):
-            s = g * per + j
-            qb[s] = (parts[t2, s].astype(F32) + ra[1, s].astype(F32)).astype(BF16)
+        for v in range(g * per, (g + 1) * per):
+            qb[v] = (parts[t2, v].astype(F32) + ra[1, v].astype(F32)).astype(BF16)
         b_copy(g).start()
 
-    @pl.loop(0, GROUPS + 2)
-    def _(it):
-        @pl.when((it < GROUPS) & (it >= (1 if per == 1 else 0)))
+    def finish(g):
+        b_copy(g).wait_recv()
+        for v in range(g * per, (g + 1) * per):
+            done = (parts[t, v].astype(F32) + ra[0, v].astype(F32) + rb[v].astype(F32)).astype(BF16)
+            if v > 0:
+                fin[v] = done
+                back(v).start()
+            else:
+                ret[0] = done
+
+    combined = [False]
+
+    def combine(g, last):
+        for v in range(g * per, (g + 1) * per):
+            if v > 0:
+                back(v).wait_recv()
+            final = last and v == (g + 1) * per - 1
+            for i in range(width // tile):
+                c = i * tile
+                term = lax.dot_general(comb[v], ret[v, :, c : c + tile], across, preferred_element_type=F32)
+                if combined[0]:
+                    term = acc[:, c : c + tile] + term
+                if final:
+                    moe_ref[:, c : c + tile] = term.astype(BF16)
+                    moe_out(i).start()
+                else:
+                    acc[:, c : c + tile] = term
+            combined[0] = True
+
+    def run(ops, last):
+        for op in ops:
+            g = int(op[1:])
+            if op[0] == "Y":
+                spread(g)
+            elif op[0] == "F":
+                forward(g)
+            elif op[0] == "M":
+                middle(g)
+            elif op[0] == "R":
+                finish(g)
+            else:
+                combine(g, last and op == ops[-1])
+
+    if per > 1:
+        spread(0)
+
+    @pl.loop(0, blocks)
+    def _(b):
+        @pl.when((b == blocks - 1) & (p > 0))
         def _():
-            for j in range(per):
-                s = it * per + j
-
-                @pl.when(s > 0)
-                def _():
-                    dispatch(s).wait_recv()
-
-            y_copy(it).start()
-            c_copy(it).start()
-
-        @pl.when((it >= 1) & (it <= GROUPS))
-        def _():
-            y_copy(it - 1).wait_recv()
-            d_copy(it - 1).start()
-
-        @pl.when(it >= 3 + LATE)
-        def _():
-            finish(it - 3)
-
-        @pl.when((it >= 2 + LATE) & (it <= GROUPS + 1))
-        def _():
-            middle(it - 2)
-
-        @pl.when(it < blocks)
-        def _():
-            @pl.when((it == blocks - 1) & (p > 0))
-            def _():
-                halo((p + 1) % n).wait_recv()
-
-            attention(blocks - 1 - it)
-
-        @pl.when(it == 1)
-        def _():
-            for load in loads:
-                load.wait()
-
-        @pl.when((it >= 1) & (it <= GROUPS))
-        def _():
-            g = it - 1
-            c_copy(g).wait_recv()
-            d_copy(g).wait_recv()
-            experts(g)
-            a_copy(0, g).start()
-            a_copy(1, g).start()
-
-    for g in reversed(range(LATE)):
-        middle(g)
-    finish(GROUPS - 1)
-    for g in reversed(range(LATE)):
-        finish(g)
-    ret[0] = fin[0]
-
-    @pl.loop(1, n)
-    def _(s):
-        back(s).wait_recv()
-
-    across = (((0,), (0,)), ((), ()))
-    for c in range(0, width, tile):
-        flat = jnp.concatenate([ret[s, :, c : c + tile].astype(F32) for s in range(n)], axis=0).astype(BF16)
-        moe_ref[:, c : c + tile] = (
-            lax.dot_general(comb[0], flat, across, preferred_element_type=F32)
-            + lax.dot_general(comb[1], flat, across, preferred_element_type=F32)
-        ).astype(BF16)
+            halo((p + 1) % n).wait_recv()
+
+        attention(blocks - 1 - b)
+
+    att_out.start()
+    for load in loads:
+        load.wait()
+
+    def step(it, code):
+        for k, ops in enumerate(PLAN):
+            @pl.when(it == k)
+            def _(ops=ops):
+                run(ops, False)
+
+        g = code % GROUPS
+        c_copy(g).wait_recv()
+        d_copy(g).wait_recv()
+        experts(g)
+        a_copy(0, g).start()
+        a_copy(1, g).start()
+        return code // GROUPS
+
+    lax.fori_loop(0, GROUPS, step, jnp.int32(sum(g * GROUPS**k for k, g in enumerate(ORDER))))
+    run(TAIL, True)
+    att_out.wait()
+    for i in range(width // tile):
+        moe_out(i).wait()
 
     @pl.when(p < n - 1)
     def _():
@@ -315,6 +342,11 @@
         a_copy(0, g).wait_send()
         a_copy(1, g).wait_send()
         b_copy(g).wait_send()
+
+
+def settle(attended_ref, moe_ref, attended_out, moe_out):
+    attended_out[...] = attended_ref[...]
+    moe_out[...] = moe_ref[...]
 
 
 def local(n, m, queries, keys_values, sinks, tokens_b, norm_gain, routes, route_weights, gate_weight, up_weight, down_weight):
@@ -329,15 +361,18 @@
     smem = pl.BlockSpec(memory_space=pltpu.SMEM)
     hbm = pl.BlockSpec(memory_space=pltpu.HBM)
     dma = pltpu.SemaphoreType.DMA
-    return pl.pallas_call(
+    attended, moe = pl.pallas_call(
         functools.partial(kernel, n, m, cap, slot_rows),
         out_shape=(
             jax.ShapeDtypeStruct(queries.shape, BF16),
             jax.ShapeDtypeStruct(tokens_b.shape, BF16),
         ),
         in_specs=[hbm, hbm, smem, vmem, vmem, vmem, vmem, hbm, hbm, hbm],
-        out_specs=(vmem, vmem),
+        out_specs=(hbm, hbm),
         scratch_shapes=[
+            pltpu.VMEM(queries.shape, BF16),
+            pltpu.VMEM(tokens_b.shape, BF16),
+            pltpu.VMEM(tokens_b.shape, F32),
             pltpu.VMEM(queries.shape, BF16),
             pltpu.VMEM((width, hid), BF16),
             pltpu.VMEM((width, hid), BF16),
@@ -353,8 +388,8 @@
             pltpu.VMEM((n, slot_rows, width), BF16),
             pltpu.VMEM((n, slot_rows, width), BF16),
             pltpu.VMEM((n, slot_rows, width), BF16),
-            pltpu.VMEM((2, n * slot_rows, own_rows), BF16),
-            dma((5,)), dma((2,)), dma((n,)), dma((n,)),
+            pltpu.VMEM((n, slot_rows, own_rows), BF16),
+            dma((1 + width // min(512, width),)), dma((5,)), dma((2,)), dma((n,)), dma((n,)),
             dma((GROUPS,)), dma((GROUPS,)), dma((GROUPS,)), dma((GROUPS,)), dma((GROUPS,)), dma((GROUPS,)),
             dma((2, GROUPS)), dma((2, GROUPS)), dma((GROUPS,)), dma((GROUPS,)), dma((n,)), dma((n,)),
         ],
@@ -373,6 +408,15 @@
         up_weight.reshape(width, hid),
         down_weight.reshape(hid, width),
     )
+    return pl.pallas_call(
+        settle,
+        out_shape=(
+            jax.ShapeDtypeStruct(queries.shape, BF16),
+            jax.ShapeDtypeStruct(tokens_b.shape, BF16),
+        ),
+        in_specs=[vmem, vmem],
+        out_specs=(vmem, vmem),
+    )(attended, moe)
 
 
 def solution(mesh):

time: 87 us -> 83.3 us (0.957)
  local copies, waits for them, and re-layouts: 3.75 us -> 0 us
    unnamed x2 -> x0, local copies, waits for them, and re-layouts: 3.75 us -> none
    pallas_call x1, Pallas kernels: 81.3 us -> 78.9 us  [local(): pl.pallas_call(functools.partial(kernel, n, m, cap, slot_rows), out_shape...]
    pallas_call x0 -> x1, Pallas kernels: none -> 2.2 us  [local(): pl.pallas_call(settle, out_shape=(jax.ShapeDtypeStruct(queries.shape, BF1...]
where the time goes in v1:
time: 83.3 us; the launch traced here: 81.7 us
  Pallas kernels  81.1 us (97%)
    pallas_call x1, Pallas kernels, local(): pl.pallas_call(functools.partial(kernel, n, m, cap, slot_rows), out_shape...  78.9 us
    pallas_call x1, Pallas kernels, local(): pl.pallas_call(settle, out_shape=(jax.ShapeDtypeStruct(queries.shape, BF1...  2.2 us

profile of v1, /device:TPU:0, one launch (start us, length us, event | category | flops | bytes accessed | tf_op | source)
XLA Modules:
  0.0 81.7 jit_solution(10531396634083959219)
XLA Ops:
  0.6 78.9 %shard_map.113 = (bf16[512,512]{1,0:T(8,128)(2,1)}, bf16[128,2048]{1,0:T(8,128)(2,1)}) custom-call(bf16[512,512]{1,0:T(8,128)(2,1)} %q_hbm.1, bf16[512,128]{1,0:T(8,128)(2,1)} %bitcast.10, f32[8]{0:T(128)} %sink_ref.1, bf16[128,2048]{1,0:T(8,128)(2,1)} %tok_ref.1, f32[1,2048]{1,0:T(1,128)} %bitcast.11, s32[2,128]{1,0:T(2,128)} %bitcast.12, ...), custom_call_target="tpu_custom_call" | custom-call | tf_op jit(solution)/shard_map/pallas_call | solution.py:364
  79.5 2.2 %shard_map.114 = (bf16[512,512]{1,0:T(8,128)(2,1)}, bf16[128,2048]{1,0:T(8,128)(2,1)}) custom-call(bf16[512,512]{1,0:T(8,128)(2,1)} %get-tuple-element.4.attended_ref, bf16[128,2048]{1,0:T(8,128)(2,1)} %get-tuple-element.5.moe_ref), custom_call_target="tpu_custom_call" | custom-call | tf_op jit(solution)/shard_map/pallas_call | solution.py:411

commit v2 on v1

--- a/solution.py
+++ b/solution.py
@@ -10,19 +10,24 @@
 WINDOW = 128
 EPSILON = 1e-06
 GROUPS = 8
-SEND = (0, 1, 4, 5, 2, 6, 3, 7)
-ORDER = (0, 1, 4, 2, 5, 3, 6, 7)
+NEAR = 4
+FAR = (4, 6, 5, 7)
+HELD = 0
+INNER = 2
+ORDER = (0, 4, 5, 1, 6, 2, 3, 7)
+HEAD = ("P0", "P1", "Y4", "P2", "P3")
 PLAN = (
-    ("Y1", "F0"),
-    ("Y4", "F1", "M0"),
-    ("Y2", "F4"),
-    ("Y5", "F2", "M4", "R0"),
-    ("Y3", "F5"),
-    ("Y6", "R4", "M5", "F3"),
-    ("Y7", "F6"),
-    ("R5", "M6", "M1", "F7"),
+    ("Y5",),
+    ("F4", "Y6"),
+    ("F5", "N1", "M4"),
+    ("N2", "F6"),
+    ("M5", "Y7", "R4"),
+    ("N3",),
+    ("M6", "R5"),
+    ("M1", "F7"),
 )
-TAIL = ("R6", "M7", "M3", "M2", "R1", "R7", "K0", "K4", "R3", "K5", "R2", "K6", "K1", "K7", "K3", "K2")
+TAIL = ("R6", "M7", "M3", "M2", "M0", "R1", "R7", "R3", "K4", "R2", "R0")
+TAIL += ("K0", "K1", "K5", "K6", "K7", "K3", "K2")
 MESH = pl.DeviceIdType.MESH
 F32 = jnp.float32
 BF16 = jnp.bfloat16
@@ -39,9 +44,10 @@
     n, m, cap, slot_rows,
     q_hbm, kv_hbm, sink_ref, tok_ref, gain_ref, routes_ref, rw_ref, wg_hbm, wu_hbm, wd_hbm,
     att_hbm, moe_hbm,
-    att_ref, moe_ref, acc, q_ref, wg, wu, wd, kvx, out, piece, xb, hidden, parts, ra, qb, rb, fin, ret, comb,
+    att_ref, moe_ref, acc, q_ref, wg, wu, wd, kvx, meta, nb, out, piece, xb, hidden, parts, ra, qb, rb, fin, ret,
+    comb, pick2,
     o_sem, w_sem, halo_sem, ep_send, ep_recv, y_send, y_recv, c_send, c_recv, d_send, d_recv,
-    a_send, a_recv, b_send, b_recv, r_send, r_recv,
+    a_send, a_recv, b_send, b_recv, r_send, r_recv, m_sem, n_send, n_recv,
 ):
     p = lax.axis_index("ep")
     t = lax.axis_index("tp")
@@ -49,7 +55,9 @@
     t2 = (t + m // 2) % m
     t3 = (t1 + m // 2) % m
     per = n // GROUPS
-    rows = m * per * slot_rows
+    near = NEAR * per
+    tc = t % 2
+    outer = 1 - (p // (n // 2) + p // (n // 4)) % 2
     width = tok_ref.shape[1]
     hid = wg.shape[1]
     row_count = q_ref.shape[0]
@@ -85,6 +93,7 @@
     normed = (widened * scale * gain_ref[...]).astype(BF16)
 
     own = normed.shape[0]
+    nb[0] = normed
     r0 = routes_ref[0:1, :]
     r1 = routes_ref[1:2, :]
     ids = lax.broadcasted_iota(jnp.int32, (max(n, 8), own), 0)
@@ -100,15 +109,26 @@
     e0 = jnp.bitwise_xor(r0, p) * slot_rows + k0
     e1 = jnp.bitwise_xor(r1, p) * slot_rows + k1
     slots = n * slot_rows
-    slot_i = lax.broadcasted_iota(jnp.int32, (slots, own), 0)
-    in0 = slot_i == e0
-    in1 = slot_i == e1
+    meta[0, 0:1] = e0.astype(F32)
+    meta[0, 1:2] = e1.astype(F32)
+    meta[0, 2:8] = jnp.zeros((6, own), F32)
+
+    def place(which, count):
+        info = meta[which]
+        slot_i = lax.broadcasted_iota(jnp.int32, (count * slot_rows, own), 0).astype(F32)
+        return slot_i == info[0:1], slot_i == info[1:2]
+
+    in0, in1 = place(0, n)
     pick = jnp.where(in0 | in1, 1.0, 0.0).astype(BF16)
     weight = jnp.where(in0, rw_ref[0:1, :], 0.0) + jnp.where(in1, rw_ref[1:2, :], 0.0)
     for s in range(n):
         comb[s] = weight[s * slot_rows : (s + 1) * slot_rows].astype(BF16)
-    def dispatch(s):
-        return remote(out.at[s], piece.at[t, s], ep_send.at[s], ep_recv.at[s], (xor(p, s), t))
+
+    def dispatch(s, half=0):
+        sem = half * n + s
+        return remote(
+            out.at[s, half], piece.at[tc, s, half], ep_send.at[sem], ep_recv.at[sem], (xor(p, s), t)
+        )
 
     def halo(to):
         return remote(kvx.at[pl.ds(row_count, WINDOW)], kvx.at[pl.ds(0, WINDOW)], halo_sem.at[0], halo_sem.at[1], (to, t))
@@ -117,17 +137,25 @@
         return pl.ds(g * per, per)
 
     def y_copy(g):
-        return remote(piece.at[t, part(g)], piece.at[t, part(g)], y_send.at[g], y_recv.at[g], (p, t2))
-
-    def c_copy(g):
-        return remote(piece.at[t, part(g)], piece.at[t, part(g)], c_send.at[g], c_recv.at[g], (p, t1))
+        return remote(piece.at[tc, part(g), 0], piece.at[tc, part(g), 1], y_send.at[g], y_recv.at[g], (p, t2))
+
+    def c_copy(g, whole):
+        here = piece.at[tc, part(g)] if whole else piece.at[tc, part(g), 0]
+        return remote(here, here, c_send.at[g], c_recv.at[g], (p, t1))
 
     tile = min(512, width)
     for c in range(0, width, tile):
         block = jnp.dot(pick, normed[:, c : c + tile], preferred_element_type=F32)
         for s in range(n):
-            out[s, :, c : c + tile] = block[s * slot_rows : (s + 1) * slot_rows].astype(BF16)
-    piece[t, 0] = out[0]
+            out[s, 0, :, c : c + tile] = block[s * slot_rows : (s + 1) * slot_rows].astype(BF16)
+    piece[tc, 0, 0] = out[0, 0]
+
+    def meta_copy():
+        return remote(meta.at[0], meta.at[1], m_sem.at[0], m_sem.at[1], (p, t2))
+
+    def token_copy(i):
+        cols = pl.ds(i * tile, tile)
+        return remote(nb.at[0, :, cols], nb.at[1, :, cols], n_send.at[i], n_recv.at[i], (p, t2))
 
     pl.semaphore_wait(barrier, n + 1)
 
@@ -137,13 +165,22 @@
     def _():
         halo(p + 1).start()
 
-    for g in SEND:
-        for v in range(max(1, g * per), (g + 1) * per):
-            dispatch(v).start()
-
-    if per == 1:
-        y_copy(0).start()
-        c_copy(0).start()
+    meta_copy().start()
+    for i in range(width // tile - HELD):
+        token_copy(i).start()
+
+    def launch(groups, half):
+        for g in groups:
+            for v in range(max(1, g * per), (g + 1) * per):
+                dispatch(v, half).start()
+
+    launch((0, 1), 0)
+
+    @pl.when(outer == 1)
+    def _():
+        launch(FAR, 0)
+
+    launch((2, 3), 0)
 
     q_load.wait()
 
@@ -152,16 +189,19 @@
         kvx[0:WINDOW, :] = jnp.zeros((WINDOW, kvx.shape[1]), BF16)
 
     def d_copy(g):
-        return remote(piece.at[t2, part(g)], piece.at[t2, part(g)], d_send.at[g], d_recv.at[g], (p, t1))
-
-    def a_copy(i, g):
-        return remote(parts.at[(t1, t3)[i], part(g)], ra.at[i, part(g)], a_send.at[i, g], a_recv.at[i, g], (p, t1))
+        return remote(piece.at[tc, part(g), 1], piece.at[tc, part(g), 1], d_send.at[g], d_recv.at[g], (p, t1))
+
+    def a_copy(g):
+        return remote(parts.at[1 - tc, part(g)], ra.at[part(g)], a_send.at[g], a_recv.at[g], (p, t1))
 
     def b_copy(g):
         return remote(qb.at[part(g)], rb.at[part(g)], b_send.at[g], b_recv.at[g], (p, t2))
 
     def back(s):
         return remote(fin.at[s], ret.at[s], r_send.at[s], r_recv.at[s], (xor(p, s), t))
+
+    def members(g):
+        return [g * per + j for j in range(per) if not (isinstance(g, int) and g * per + j == 0)]
 
     def attention(b):
         head = kvx.shape[1] // 2
@@ -202,7 +242,7 @@
         for o in range(m):
             for j in range(0, per):
                 k = (o * per + j) * slot_rows
-                xb[k : k + slot_rows, :] = piece[o, g * per + j]
+                xb[k : k + slot_rows, :] = piece[o // 2, g * per + j, o % 2]
         full = hid // 256 * 256
         x = xb[...]
         for c in range(0, full, 256):
@@ -221,7 +261,7 @@
             for o in range(m):
                 for j in range(per):
                     k = (o * per + j) * slot_rows
-                    parts[o, g * per + j, :, c : c + 256] = product[k : k + slot_rows].astype(BF16)
+                    parts[o // 2, g * per + j, o % 2, :, c : c + 256] = product[k : k + slot_rows].astype(BF16)
 
     across = (((0,), (0,)), ((), ()))
     att_out = pltpu.make_async_copy(att_ref, att_hbm, o_sem.at[0])
@@ -230,68 +270,107 @@
         cols = pl.ds(i * tile, tile)
         return pltpu.make_async_copy(moe_ref.at[:, cols], moe_hbm.at[:, cols], o_sem.at[1 + i])
 
+    def peer(i):
+        c = i * tile
+        if i == 0:
+            meta_copy().wait_recv()
+            one0, one1 = place(1, near)
+            pick2[0] = jnp.where(one0 | one1, 1.0, 0.0).astype(BF16)
+        token_copy(i).wait_recv()
+        block = jnp.dot(pick2[0], nb[1, :, c : c + tile], preferred_element_type=F32)
+        for v in range(near):
+            rows = block[v * slot_rows : (v + 1) * slot_rows].astype(BF16)
+            if v > 0:
+                out[v, 1, :, c : c + tile] = rows
+            else:
+                piece[tc, 0, 1, :, c : c + tile] = rows
+        if i == INNER:
+            @pl.when(outer == 0)
+            def _():
+                launch(FAR, 0)
+
+        if i == width // tile - 1:
+            launch((0, 1, 2, 3), 1)
+            gather(0)
+
+    def queue(i):
+        token_copy(i).start()
+
+    def gather(g):
+        for v in members(g):
+            dispatch(v).wait_recv()
+            dispatch(v, 1).wait_recv()
+        c_copy(g, True).start()
+
     def spread(g):
-        for v in range(max(1, g * per), (g + 1) * per):
+        for v in members(g):
             dispatch(v).wait_recv()
         y_copy(g).start()
-        c_copy(g).start()
+        c_copy(g, False).start()
 
     def forward(g):
         y_copy(g).wait_recv()
         d_copy(g).start()
 
     def middle(g):
-        a_copy(0, g).wait_recv()
-        a_copy(1, g).wait_recv()
-        for v in range(g * per, (g + 1) * per):
-            qb[v] = (parts[t2, v].astype(F32) + ra[1, v].astype(F32)).astype(BF16)
+        a_copy(g).wait_recv()
+        for j in range(per):
+            v = g * per + j
+            qb[v] = (parts[tc, v, 1].astype(F32) + ra[v, 1].astype(F32)).astype(BF16)
         b_copy(g).start()
 
     def finish(g):
         b_copy(g).wait_recv()
-        for v in range(g * per, (g + 1) * per):
-            done = (parts[t, v].astype(F32) + ra[0, v].astype(F32) + rb[v].astype(F32)).astype(BF16)
-            if v > 0:
+        for j in range(per):
+            v = g * per + j
+            done = (parts[tc, v, 0].astype(F32) + ra[v, 0].astype(F32) + rb[v].astype(F32)).astype(BF16)
+            if isinstance(v, int) and v == 0:
+                ret[0] = done
+            else:
                 fin[v] = done
                 back(v).start()
-            else:
-                ret[0] = done
-
-    combined = [False]
+
+    def actual(g):
+        return g + (g // NEAR) * 2 * outer * (1 - 2 * ((g // 2) % 2))
+
+    begun = [False]
 
     def combine(g, last):
-        for v in range(g * per, (g + 1) * per):
-            if v > 0:
+        for j in range(per):
+            v = g * per + j
+            if not (isinstance(v, int) and v == 0):
                 back(v).wait_recv()
-            final = last and v == (g + 1) * per - 1
             for i in range(width // tile):
-                c = i * tile
-                term = lax.dot_general(comb[v], ret[v, :, c : c + tile], across, preferred_element_type=F32)
-                if combined[0]:
-                    term = acc[:, c : c + tile] + term
-                if final:
-                    moe_ref[:, c : c + tile] = term.astype(BF16)
+                cols = slice(i * tile, (i + 1) * tile)
+                term = lax.dot_general(comb[v], ret[v, :, cols], across, preferred_element_type=F32)
+                if begun[0]:
+                    term = acc[:, cols] + term
+                if last and j == per - 1:
+                    moe_ref[:, cols] = term.astype(BF16)
                     moe_out(i).start()
                 else:
-                    acc[:, c : c + tile] = term
-            combined[0] = True
-
-    def run(ops, last):
+                    acc[:, cols] = term
+            begun[0] = True
+
+    def arrive(g, close):
+        c_copy(g, close).wait_recv()
+        if not close:
+            d_copy(g).wait_recv()
+
+    acts = dict(P=peer, Q=queue, N=gather, Y=spread, F=forward, M=middle, R=finish)
+
+    def run(ops, last=False):
         for op in ops:
             g = int(op[1:])
-            if op[0] == "Y":
-                spread(g)
-            elif op[0] == "F":
-                forward(g)
-            elif op[0] == "M":
-                middle(g)
-            elif op[0] == "R":
-                finish(g)
+            close = g < NEAR
+            final = last and op == ops[-1]
+            where = g if close else actual(g)
+            if op[0] == "K":
+                combine(where, final)
+            elif op[0] == "E":
+                arrive(where, close)
             else:
-                combine(g, last and op == ops[-1])
-
-    if per > 1:
-        spread(0)
+                acts[op[0]](where)
 
     @pl.loop(0, blocks)
     def _(b):
@@ -305,18 +384,17 @@
     for load in loads:
         load.wait()
 
+    run(HEAD)
+
     def step(it, code):
         for k, ops in enumerate(PLAN):
             @pl.when(it == k)
-            def _(ops=ops):
-                run(ops, False)
-
-        g = code % GROUPS
-        c_copy(g).wait_recv()
-        d_copy(g).wait_recv()
+            def _(ops=ops + ("E%d" % ORDER[k],)):
+                run(ops)
+
+        g = actual(code % GROUPS)
         experts(g)
-        a_copy(0, g).start()
-        a_copy(1, g).start()
+        a_copy(g).start()
         return code // GROUPS
 
     lax.fori_loop(0, GROUPS, step, jnp.int32(sum(g * GROUPS**k for k, g in enumerate(ORDER))))
@@ -329,19 +407,21 @@
     def _():
         halo(p + 1).wait_send()
 
-    @pl.loop(1, n)
-    def _(s):
+    meta_copy().wait_send()
+    for i in range(width // tile):
+        token_copy(i).wait_send()
+    for s in range(1, n):
         dispatch(s).wait_send()
         back(s).wait_send()
-
-    @pl.loop(0, GROUPS)
-    def _(g):
-        y_copy(g).wait_send()
-        c_copy(g).wait_send()
-        d_copy(g).wait_send()
-        a_copy(0, g).wait_send()
-        a_copy(1, g).wait_send()
+        if s < near:
+            dispatch(s, 1).wait_send()
+    for g in range(GROUPS):
+        c_copy(g, g < NEAR).wait_send()
+        a_copy(g).wait_send()
         b_copy(g).wait_send()
+        if g >= NEAR:
+            y_copy(g).wait_send()
+            d_copy(g).wait_send()
 
 
 def settle(attended_ref, moe_ref, attended_out, moe_out):
@@ -357,6 +437,7 @@
     hid = gate_weight.shape[2]
     per = n // GROUPS
     rows = m * per * slot_rows
+    tiles = width // min(512, width)
     vmem = pl.BlockSpec(memory_space=pltpu.VMEM)
     smem = pl.BlockSpec(memory_space=pltpu.SMEM)
     hbm = pl.BlockSpec(memory_space=pltpu.HBM)
@@ -378,20 +459,24 @@
             pltpu.VMEM((width, hid), BF16),
             pltpu.VMEM((hid, width), BF16),
             pltpu.VMEM((keys_values.shape[0] + WINDOW, keys_values.shape[2]), BF16),
-            pltpu.VMEM((n, slot_rows, width), BF16),
-            pltpu.VMEM((m, n, slot_rows, width), BF16),
+            pltpu.VMEM((2, 8, own_rows), F32),
+            pltpu.VMEM((2, own_rows, width), BF16),
+            pltpu.VMEM((n, 2, slot_rows, width), BF16),
+            pltpu.VMEM((2, n, 2, slot_rows, width), BF16),
             pltpu.VMEM((rows, width), BF16),
             pltpu.VMEM((rows, hid), BF16),
-            pltpu.VMEM((m, n, slot_rows, width), BF16),
-            pltpu.VMEM((2, n, slot_rows, width), BF16),
+            pltpu.VMEM((2, n, 2, slot_rows, width), BF16),
+            pltpu.VMEM((n, 2, slot_rows, width), BF16),
             pltpu.VMEM((n, slot_rows, width), BF16),
             pltpu.VMEM((n, slot_rows, width), BF16),
             pltpu.VMEM((n, slot_rows, width), BF16),
             pltpu.VMEM((n, slot_rows, width), BF16),
             pltpu.VMEM((n, slot_rows, own_rows), BF16),
-            dma((1 + width // min(512, width),)), dma((5,)), dma((2,)), dma((n,)), dma((n,)),
+            pltpu.VMEM((1, NEAR * per * slot_rows, own_rows), BF16),
+            dma((1 + tiles,)), dma((5,)), dma((2,)), dma((2 * n,)), dma((2 * n,)),
             dma((GROUPS,)), dma((GROUPS,)), dma((GROUPS,)), dma((GROUPS,)), dma((GROUPS,)), dma((GROUPS,)),
-            dma((2, GROUPS)), dma((2, GROUPS)), dma((GROUPS,)), dma((GROUPS,)), dma((n,)), dma((n,)),
+            dma((GROUPS,)), dma((GROUPS,)), dma((GROUPS,)), dma((GROUPS,)), dma((n,)), dma((n,)),
+            dma((2,)), dma((tiles,)), dma((tiles,)),
         ],
         compiler_params=pltpu.CompilerParams(
             collective_id=0, has_side_effects=True, vmem_limit_bytes=62 * 1024 * 1024

time: 83.3 us -> 76.6 us (0.920)
  Pallas kernels: 81.1 us -> 74.9 us
    pallas_call x1, Pallas kernels: 78.9 us -> 72.7 us  [local(): pl.pallas_call(functools.partial(kernel, n, m, cap, slot_rows), out_shape...]
where the time goes in v2:
time: 76.6 us; the launch traced here: 75.6 us
  Pallas kernels  74.9 us (98%)
    pallas_call x1, Pallas kernels, local(): pl.pallas_call(functools.partial(kernel, n, m, cap, slot_rows), out_shape...  72.7 us
    pallas_call x1, Pallas kernels, local(): pl.pallas_call(settle, out_shape=(jax.ShapeDtypeStruct(queries.shape, BF1...  2.2 us

profile of v2, /device:TPU:0, one launch (start us, length us, event | category | flops | bytes accessed | tf_op | source)
XLA Modules:
  0.0 75.6 jit_solution(11316969645553589504)
XLA Ops:
  0.6 72.7 %shard_map.113 = (bf16[512,512]{1,0:T(8,128)(2,1)}, bf16[128,2048]{1,0:T(8,128)(2,1)}) custom-call(bf16[512,512]{1,0:T(8,128)(2,1)} %q_hbm.1, bf16[512,128]{1,0:T(8,128)(2,1)} %bitcast.10, f32[8]{0:T(128)} %sink_ref.1, bf16[128,2048]{1,0:T(8,128)(2,1)} %tok_ref.1, f32[1,2048]{1,0:T(1,128)} %bitcast.11, s32[2,128]{1,0:T(2,128)} %bitcast.12, ...), custom_call_target="tpu_custom_call" | custom-call | tf_op jit(solution)/shard_map/pallas_call | solution.py:445
  73.4 2.2 %shard_map.114 = (bf16[512,512]{1,0:T(8,128)(2,1)}, bf16[128,2048]{1,0:T(8,128)(2,1)}) custom-call(bf16[512,512]{1,0:T(8,128)(2,1)} %get-tuple-element.4.attended_ref, bf16[128,2048]{1,0:T(8,128)(2,1)} %get-tuple-element.5.moe_ref), custom_call_target="tpu_custom_call" | custom-call | tf_op jit(solution)/shard_map/pallas_call | solution.py:496

commit v3 on v2

--- a/solution.py
+++ b/solution.py
@@ -11,7 +11,9 @@
 EPSILON = 1e-06
 GROUPS = 8
 NEAR = 4
-FAR = (4, 6, 5, 7)
+OUTER_FAR = (6, 4, 5, 7)
+INNER_FAR = (4, 6, 7, 5)
+PARTS = 2
 HELD = 0
 INNER = 2
 ORDER = (0, 4, 5, 1, 6, 2, 3, 7)
@@ -23,11 +25,11 @@
     ("N2", "F6"),
     ("M5", "Y7", "R4"),
     ("N3",),
-    ("M6", "R5"),
+    ("R5", "M6"),
     ("M1", "F7"),
 )
-TAIL = ("R6", "M7", "M3", "M2", "M0", "R1", "R7", "R3", "K4", "R2", "R0")
-TAIL += ("K0", "K1", "K5", "K6", "K7", "K3", "K2")
+TAIL = ("R6", "M7", "M3", "M2", "M0", "R1", "R7", "R3", "K4")
+TAIL += ("R2", "R0", "S0", "K0", "K1", "K5", "K6", "K7", "K3", "K2")
 MESH = pl.DeviceIdType.MESH
 F32 = jnp.float32
 BF16 = jnp.bfloat16
@@ -42,8 +44,9 @@
 
 def kernel(
     n, m, cap, slot_rows,
-    q_hbm, kv_hbm, sink_ref, tok_ref, gain_ref, routes_ref, rw_ref, wg_hbm, wu_hbm, wd_hbm,
+    q_hbm, kv_hbm, sink_hbm, tok_hbm, gain_hbm, routes_hbm, rw_hbm, wg_hbm, wu_hbm, wd_hbm,
     att_hbm, moe_hbm,
+    sink_ref, tok_ref, gain_ref, routes_ref, rw_ref, i_sem,
     att_ref, moe_ref, acc, q_ref, wg, wu, wd, kvx, meta, nb, out, piece, xb, hidden, parts, ra, qb, rb, fin, ret,
     comb, pick2,
     o_sem, w_sem, halo_sem, ep_send, ep_recv, y_send, y_recv, c_send, c_recv, d_send, d_recv,
@@ -57,6 +60,7 @@
     per = n // GROUPS
     near = NEAR * per
     tc = t % 2
+    part_width = tok_ref.shape[1] // PARTS
     outer = 1 - (p // (n // 2) + p // (n // 4)) % 2
     width = tok_ref.shape[1]
     hid = wg.shape[1]
@@ -77,6 +81,14 @@
     ]
     q_load = pltpu.make_async_copy(q_hbm, q_ref, w_sem.at[3])
     kv_load = pltpu.make_async_copy(kv_hbm, kvx.at[pl.ds(WINDOW, row_count)], w_sem.at[4])
+    early = [
+        pltpu.make_async_copy(source, target, i_sem.at[i])
+        for i, (source, target) in enumerate((
+            (tok_hbm, tok_ref), (gain_hbm, gain_ref), (routes_hbm, routes_ref), (rw_hbm, rw_ref), (sink_hbm, sink_ref),
+        ))
+    ]
+    for load in early:
+        load.start()
     barrier = pltpu.get_barrier_semaphore()
     for s in range(1, n):
         pl.semaphore_signal(barrier, inc=1, device_id=(xor(p, s), t), device_id_type=MESH)
@@ -88,6 +100,8 @@
     for load in loads:
         load.start()
 
+    for load in early:
+        load.wait()
     widened = tok_ref[...].astype(F32)
     scale = lax.rsqrt(jnp.mean(widened * widened, axis=-1, keepdims=True) + EPSILON)
     normed = (widened * scale * gain_ref[...]).astype(BF16)
@@ -178,7 +192,7 @@
 
     @pl.when(outer == 1)
     def _():
-        launch(FAR, 0)
+        launch(OUTER_FAR, 0)
 
     launch((2, 3), 0)
 
@@ -194,11 +208,17 @@
     def a_copy(g):
         return remote(parts.at[1 - tc, part(g)], ra.at[part(g)], a_send.at[g], a_recv.at[g], (p, t1))
 
-    def b_copy(g):
-        return remote(qb.at[part(g)], rb.at[part(g)], b_send.at[g], b_recv.at[g], (p, t2))
-
-    def back(s):
-        return remote(fin.at[s], ret.at[s], r_send.at[s], r_recv.at[s], (xor(p, s), t))
+    def b_copy(g, h):
+        cols = pl.ds(h * part_width, part_width)
+        return remote(
+            qb.at[part(g), :, cols], rb.at[part(g), :, cols], b_send.at[h, g], b_recv.at[h, g], (p, t2)
+        )
+
+    def back(s, h):
+        cols = pl.ds(h * part_width, part_width)
+        return remote(
+            fin.at[s, :, cols], ret.at[s, :, cols], r_send.at[h, s], r_recv.at[h, s], (xor(p, s), t)
+        )
 
     def members(g):
         return [g * per + j for j in range(per) if not (isinstance(g, int) and g * per + j == 0)]
@@ -287,7 +307,7 @@
         if i == INNER:
             @pl.when(outer == 0)
             def _():
-                launch(FAR, 0)
+                launch(INNER_FAR, 0)
 
         if i == width // tile - 1:
             launch((0, 1, 2, 3), 1)
@@ -314,21 +334,27 @@
 
     def middle(g):
         a_copy(g).wait_recv()
-        for j in range(per):
-            v = g * per + j
-            qb[v] = (parts[tc, v, 1].astype(F32) + ra[v, 1].astype(F32)).astype(BF16)
-        b_copy(g).start()
+        for h in range(PARTS):
+            cols = slice(h * part_width, (h + 1) * part_width)
+            for j in range(per):
+                v = g * per + j
+                mine = parts[tc, v, 1, :, cols].astype(F32)
+                qb[v, :, cols] = (mine + ra[v, 1, :, cols].astype(F32)).astype(BF16)
+            b_copy(g, h).start()
 
     def finish(g):
-        b_copy(g).wait_recv()
-        for j in range(per):
-            v = g * per + j
-            done = (parts[tc, v, 0].astype(F32) + ra[v, 0].astype(F32) + rb[v].astype(F32)).astype(BF16)
-            if isinstance(v, int) and v == 0:
-                ret[0] = done
-            else:
-                fin[v] = done
-                back(v).start()
+        for h in range(PARTS):
+            cols = slice(h * part_width, (h + 1) * part_width)
+            b_copy(g, h).wait_recv()
+            for j in range(per):
+                v = g * per + j
+                mine = parts[tc, v, 0, :, cols].astype(F32) + ra[v, 0, :, cols].astype(F32)
+                done = (mine + rb[v, :, cols].astype(F32)).astype(BF16)
+                if isinstance(v, int) and v == 0:
+                    ret[0, :, cols] = done
+                else:
+                    fin[v, :, cols] = done
+                    back(v, h).start()
 
     def actual(g):
         return g + (g // NEAR) * 2 * outer * (1 - 2 * ((g // 2) % 2))
@@ -338,9 +364,9 @@
     def combine(g, last):
         for j in range(per):
             v = g * per + j
-            if not (isinstance(v, int) and v == 0):
-                back(v).wait_recv()
             for i in range(width // tile):
+                if not (isinstance(v, int) and v == 0) and i * tile % part_width == 0:
+                    back(v, i * tile // part_width).wait_recv()
                 cols = slice(i * tile, (i + 1) * tile)
                 term = lax.dot_general(comb[v], ret[v, :, cols], across, preferred_element_type=F32)
                 if begun[0]:
@@ -357,7 +383,28 @@
         if not close:
             d_copy(g).wait_recv()
 
-    acts = dict(P=peer, Q=queue, N=gather, Y=spread, F=forward, M=middle, R=finish)
+    def drain(_):
+        @pl.when(p < n - 1)
+        def _():
+            halo(p + 1).wait_send()
+
+        meta_copy().wait_send()
+        for i in range(width // tile):
+            token_copy(i).wait_send()
+        for s in range(1, n):
+            dispatch(s).wait_send()
+            if s < near:
+                dispatch(s, 1).wait_send()
+        for g in range(GROUPS):
+            c_copy(g, g < NEAR).wait_send()
+            a_copy(g).wait_send()
+            for h in range(PARTS):
+                b_copy(g, h).wait_send()
+            if g >= NEAR:
+                y_copy(g).wait_send()
+                d_copy(g).wait_send()
+
+    acts = dict(S=drain, P=peer, Q=queue, N=gather, Y=spread, F=forward, M=middle, R=finish)
 
     def run(ops, last=False):
         for op in ops:
@@ -403,30 +450,26 @@
     for i in range(width // tile):
         moe_out(i).wait()
 
-    @pl.when(p < n - 1)
-    def _():
-        halo(p + 1).wait_send()
-
-    meta_copy().wait_send()
-    for i in range(width // tile):
-        token_copy(i).wait_send()
     for s in range(1, n):
-        dispatch(s).wait_send()
-        back(s).wait_send()
-        if s < near:
-            dispatch(s, 1).wait_send()
-    for g in range(GROUPS):
-        c_copy(g, g < NEAR).wait_send()
-        a_copy(g).wait_send()
-        b_copy(g).wait_send()
-        if g >= NEAR:
-            y_copy(g).wait_send()
-            d_copy(g).wait_send()
-
-
-def settle(attended_ref, moe_ref, attended_out, moe_out):
-    attended_out[...] = attended_ref[...]
-    moe_out[...] = moe_ref[...]
+        for h in range(PARTS):
+            back(s, h).wait_send()
+
+
+def settle(attended_hbm, moe_hbm, attended_out, moe_out, attended_ref, moe_ref, sem):
+    loads, stores = [], []
+    for source, held, target in ((attended_hbm, attended_ref, attended_out), (moe_hbm, moe_ref, moe_out)):
+        step = source.shape[0] // 2
+        for i in range(2):
+            at = pl.ds(i * step, step)
+            loads.append(pltpu.make_async_copy(source.at[at], held.at[at], sem.at[0, len(loads)]))
+            stores.append(pltpu.make_async_copy(held.at[at], target.at[at], sem.at[1, len(stores)]))
+    for load in loads:
+        load.start()
+    for load, store in zip(loads, stores):
+        load.wait()
+        store.start()
+    for store in stores:
+        store.wait()
 
 
 def local(n, m, queries, keys_values, sinks, tokens_b, norm_gain, routes, route_weights, gate_weight, up_weight, down_weight):
@@ -438,8 +481,6 @@
     per = n // GROUPS
     rows = m * per * slot_rows
     tiles = width // min(512, width)
-    vmem = pl.BlockSpec(memory_space=pltpu.VMEM)
-    smem = pl.BlockSpec(memory_space=pltpu.SMEM)
     hbm = pl.BlockSpec(memory_space=pltpu.HBM)
     dma = pltpu.SemaphoreType.DMA
     attended, moe = pl.pallas_call(
@@ -448,9 +489,15 @@
             jax.ShapeDtypeStruct(queries.shape, BF16),
             jax.ShapeDtypeStruct(tokens_b.shape, BF16),
         ),
-        in_specs=[hbm, hbm, smem, vmem, vmem, vmem, vmem, hbm, hbm, hbm],
+        in_specs=[hbm] * 10,
         out_specs=(hbm, hbm),
         scratch_shapes=[
+            pltpu.SMEM(sinks.shape, F32),
+            pltpu.VMEM(tokens_b.shape, BF16),
+            pltpu.VMEM((1, width), F32),
+            pltpu.VMEM((top_count, own_rows), jnp.int32),
+            pltpu.VMEM((top_count, own_rows), F32),
+            dma((5,)),
             pltpu.VMEM(queries.shape, BF16),
             pltpu.VMEM(tokens_b.shape, BF16),
             pltpu.VMEM(tokens_b.shape, F32),
@@ -475,7 +522,8 @@
             pltpu.VMEM((1, NEAR * per * slot_rows, own_rows), BF16),
             dma((1 + tiles,)), dma((5,)), dma((2,)), dma((2 * n,)), dma((2 * n,)),
             dma((GROUPS,)), dma((GROUPS,)), dma((GROUPS,)), dma((GROUPS,)), dma((GROUPS,)), dma((GROUPS,)),
-            dma((GROUPS,)), dma((GROUPS,)), dma((GROUPS,)), dma((GROUPS,)), dma((n,)), dma((n,)),
+            dma((GROUPS,)), dma((GROUPS,)), dma((PARTS, GROUPS)), dma((PARTS, GROUPS)),
+            dma((PARTS, n)), dma((PARTS, n)),
             dma((2,)), dma((tiles,)), dma((tiles,)),
         ],
         compiler_params=pltpu.CompilerParams(
@@ -499,8 +547,13 @@
             jax.ShapeDtypeStruct(queries.shape, BF16),
             jax.ShapeDtypeStruct(tokens_b.shape, BF16),
         ),
-        in_specs=[vmem, vmem],
-        out_specs=(vmem, vmem),
+        in_specs=[hbm, hbm],
+        out_specs=(hbm, hbm),
+        scratch_shapes=[
+            pltpu.VMEM(queries.shape, BF16),
+            pltpu.VMEM(tokens_b.shape, BF16),
+            dma((2, 4)),
+        ],
     )(attended, moe)
 
 

time: 76.6 us -> 74.1 us (0.967); the launches traced: 75.6 us -> 74 us
  Pallas kernels: 74.9 us -> 73.3 us
    pallas_call x1, Pallas kernels: 72.7 us -> 71.4 us  [local(): pl.pallas_call(functools.partial(kernel, n, m, cap, slot_rows), out_shape...]
where the time goes in v3:
time: 74.1 us; the launch traced here: 74 us
  Pallas kernels  73.3 us (99%)
    pallas_call x1, Pallas kernels, local(): pl.pallas_call(functools.partial(kernel, n, m, cap, slot_rows), out_shape...  71.4 us
    pallas_call x1, Pallas kernels, local(): pl.pallas_call(settle, out_shape=(jax.ShapeDtypeStruct(queries.shape, BF1...  1.98 us

profile of v3, /device:TPU:0, one launch (start us, length us, event | category | flops | bytes accessed | tf_op | source)
XLA Modules:
  0.0 74.0 jit_solution(16420078290615284600)
XLA Ops:
  0.6 71.4 %shard_map.113 = (bf16[512,512]{1,0:T(8,128)(2,1)}, bf16[128,2048]{1,0:T(8,128)(2,1)}) custom-call(bf16[512,512]{1,0:T(8,128)(2,1)} %q_hbm.1, bf16[512,128]{1,0:T(8,128)(2,1)} %bitcast.10, f32[8]{0:T(128)} %sink_hbm.1, bf16[128,2048]{1,0:T(8,128)(2,1)} %tok_hbm.1, f32[1,2048]{1,0:T(1,128)} %bitcast.11, s32[2,128]{1,0:T(2,128)} %bitcast.12, ...), custom_call_target="tpu_custom_call" | custom-call | tf_op jit(solution)/shard_map/pallas_call | solution.py:486
  72.0 2.0 %shard_map.114 = (bf16[512,512]{1,0:T(8,128)(2,1)}, bf16[128,2048]{1,0:T(8,128)(2,1)}) custom-call(bf16[512,512]{1,0:T(8,128)(2,1)} %get-tuple-element.4.attended_hbm, bf16[128,2048]{1,0:T(8,128)(2,1)} %get-tuple-element.5.moe_hbm), custom_call_target="tpu_custom_call" | custom-call | tf_op jit(solution)/shard_map/pallas_call | solution.py:544

commit v4 on v3

--- a/solution.py
+++ b/solution.py
@@ -25,7 +25,7 @@
     ("N2", "F6"),
     ("M5", "Y7", "R4"),
     ("N3",),
-    ("R5", "M6"),
+    ("M6", "R5"),
     ("M1", "F7"),
 )
 TAIL = ("R6", "M7", "M3", "M2", "M0", "R1", "R7", "R3", "K4")

time: 74.1 us -> 74.1 us (level)
  no operation moved by 1% of the time
where the time goes in v4:
time: 74.1 us; the launch traced here: 74 us
  Pallas kernels  73.4 us (99%)
    pallas_call x1, Pallas kernels, local(): pl.pallas_call(functools.partial(kernel, n, m, cap, slot_rows), out_shape...  71.4 us
    pallas_call x1, Pallas kernels, local(): pl.pallas_call(settle, out_shape=(jax.ShapeDtypeStruct(queries.shape, BF1...  1.98 us

profile of v4, /device:TPU:0, one launch (start us, length us, event | category | flops | bytes accessed | tf_op | source)
XLA Modules:
  0.0 74.0 jit_solution(3600233328595151527)
XLA Ops:
  0.6 71.4 %shard_map.113 = (bf16[512,512]{1,0:T(8,128)(2,1)}, bf16[128,2048]{1,0:T(8,128)(2,1)}) custom-call(bf16[512,512]{1,0:T(8,128)(2,1)} %q_hbm.1, bf16[512,128]{1,0:T(8,128)(2,1)} %bitcast.10, f32[8]{0:T(128)} %sink_hbm.1, bf16[128,2048]{1,0:T(8,128)(2,1)} %tok_hbm.1, f32[1,2048]{1,0:T(1,128)} %bitcast.11, s32[2,128]{1,0:T(2,128)} %bitcast.12, ...), custom_call_target="tpu_custom_call" | custom-call | tf_op jit(solution)/shard_map/pallas_call | solution.py:486
  72.0 2.0 %shard_map.114 = (bf16[512,512]{1,0:T(8,128)(2,1)}, bf16[128,2048]{1,0:T(8,128)(2,1)}) custom-call(bf16[512,512]{1,0:T(8,128)(2,1)} %get-tuple-element.4.attended_hbm, bf16[128,2048]{1,0:T(8,128)(2,1)} %get-tuple-element.5.moe_hbm), custom_call_target="tpu_custom_call" | custom-call | tf_op jit(solution)/shard_map/pallas_call | solution.py:544
